TPU v7x, 128 devices: a whole 4x4x4 slice. The times are simulated.
128 devices in a mesh: sp: 32 (over z, y, core), tp: 4 (over x).
Axes of the slice: x: 4, y: 4, z: 4, core: 2. Of those that a mesh axis runs over, the one named last changes fastest.
Arguments:
- residual: bfloat16 [32768, 2048], P('sp'), may hold values from -6 to 6
- small_heads: bfloat16 [32768, 1024], P('sp', 'tp'), may hold values from -6 to 6
- large_heads: bfloat16 [32768, 1024], P('sp', 'tp'), may hold values from -6 to 6
- state_keys: bfloat16 [32768, 8, 128], P('sp', 'tp'), may hold values from -6 to 6
- state_queries: bfloat16 [32768, 8, 128], P('sp', 'tp'), may hold values from -6 to 6
- small_gate: bfloat16 [32768, 1024], P('sp', 'tp'), may hold values from -6 to 6
- large_gate: bfloat16 [32768, 1024], P('sp', 'tp'), may hold values from -6 to 6
- small_step: float32 [32768, 16], P('sp', 'tp'), may hold values from -3 to 2
- large_step: float32 [32768, 8], P('sp', 'tp'), may hold values from -3 to 2
- small_taps: bfloat16 [4, 1024], P(None, 'tp'), may hold values from -3 to 3
- large_taps: bfloat16 [4, 1024], P(None, 'tp'), may hold values from -3 to 3
- key_taps: bfloat16 [4, 8, 128], P(None, 'tp'), may hold values from -3 to 3
- query_taps: bfloat16 [4, 8, 128], P(None, 'tp'), may hold values from -3 to 3
- small_decay: float32 [16], P('tp'), may hold values from -12 to -2, as said below
- large_decay: float32 [8], P('tp'), may hold values from -12 to -2, as said below
- small_gain: bfloat16 [1024], P('tp'), may hold values from 0.099609375 to 1.8984375
- large_gain: bfloat16 [1024], P('tp'), may hold values from 0.099609375 to 1.8984375
- small_out: bfloat16 [1024, 2048], P('tp'), may hold values from -0.125 to 0.125
- large_out: bfloat16 [1024, 2048], P('tp'), may hold values from -0.125 to 0.125
- mixer_gain: bfloat16 [2048], replicated, may hold values from 0.099609375 to 1.8984375
- ffn_in_gain: bfloat16 [2048], replicated, may hold values from 0.099609375 to 1.8984375
- gate_proj: bfloat16 [2048, 5632], P('sp', 'tp'), may hold values from -0.125 to 0.125
- up_proj: bfloat16 [2048, 5632], P('sp', 'tp'), may hold values from -0.125 to 0.125
- down_proj: bfloat16 [2048, 5632], P('sp', 'tp'), may hold values from -0.078125 to 0.078125
- ffn_out_gain: bfloat16 [2048], replicated, may hold values from 0.099609375 to 1.8984375
Outputs:
- updated: bfloat16 [32768, 2048], P(('sp', 'tp'))
Inputs may be any that keep to these rules, and one draw needn't show every extreme that they name: `small_decay`: log decay rates of the first group. `large_decay`: log decay rates of the second group.
All inputs are finite; a program needn't handle non-finite values.
Results may differ from a plain program's by a relative error of at most 0.014.
Values may be sent and summed in bfloat16 or wider, within the bound.
No kernel may reach another device: no remote copies, remote signals or barrier semaphores. Data moves between devices by JAX's collectives and lax.ppermute only.
A program may use at most 192 MiB of HBM per device.

v0:
```python
import jax
import jax.numpy as jnp
from jax import lax
from jax.sharding import Mesh
from jax.sharding import PartitionSpec as P

BLOCK = 128
SP = ("sp_0", "sp_1", "sp_2")
SP_TP = ("sp_0", "sp_1", "sp_2", "tp")
EPS = 1e-06


def passed_along(block, axis, distance):
    devices = range(lax.axis_size(axis))
    route = [(i - distance, i) for i in devices if i - distance in devices]
    return lax.ppermute(block, axis, route)


def nothing_yet(array, identity):
    return jax.tree.map(
        lambda a, e: jnp.broadcast_to(jnp.asarray(e, a.dtype), a.shape), array, identity
    )


def collected_together(array, axis):
    leaves = jax.tree.leaves(array)
    sequence = sorted(range(len(leaves)), key=lambda k: -leaves[k].size)
    width = (1, *leaves[sequence[0]].shape)[-1]
    lines = [
        jnp.pad(leaves[k].reshape(-1), (0, -leaves[k].size % width)).reshape(-1, width)
        for k in sequence
    ]
    both, at, found = (lax.all_gather(jnp.concatenate(lines), axis), 0, {})
    for k, line in zip(sequence, lines):
        slab = both[:, at : at + len(line)].reshape(len(both), -1)
        found[k] = slab[:, : leaves[k].size].reshape(-1, *leaves[k].shape)
        at += len(line)
    numbers = iter(range(len(leaves)))
    return jax.tree.map(lambda _: found[next(numbers)], array)


def prefix_by_axis(array, axes, combine, identity):
    before = start = nothing_yet(array, identity)
    subtotal = array
    for axis in reversed(axes):
        peers, position = (lax.axis_size(axis), lax.axis_index(axis))
        pieces = collected_together(
            jax.tree.map(
                lambda part, kind: part.astype(kind),
                subtotal,
                (jnp.bfloat16, jnp.bfloat16, jnp.bfloat16, jnp.bfloat16),
            ),
            axis,
        )
        inside, subtotal = (start, start)
        for k in range(peers):
            passed = k < position
            subtotal = combine(
                subtotal, jax.tree.map(lambda part, own: part[k].astype(own.dtype), pieces, array)
            )
            inside = jax.tree.map(lambda new, old: jnp.where(passed, new, old), subtotal, inside)
        before = combine(inside, before)
    return before


def in_one_piece(arrays, axis, dim, along):
    both = jnp.concatenate(arrays, axis=along)
    whole, at, finished = (lax.all_gather(both, axis, axis=dim, tiled=True), 0, [])
    for a in arrays:
        finished.append(lax.slice_in_dim(whole, at, at + a.shape[along], axis=along))
        at += a.shape[along]
    return tuple(finished)


def in_order(pieces, dim):
    pieces = jnp.moveaxis(pieces, 0, dim)
    dims = pieces.shape
    return pieces.reshape(*dims[:dim], dims[dim] * dims[dim + 1], *dims[dim + 2 :])


def all_blocks(array, axes, sequence):
    pieces = array
    for k in sequence:
        pieces = lax.all_gather(pieces, axes[k])
    done = sequence[::-1]
    back = [done.index(k) for k in range(len(axes))]
    pieces = pieces.transpose(*back, *range(len(axes), pieces.ndim))
    return pieces.reshape(-1, *array.shape)


def gather_axes(array, axes, sequence, dim):
    return in_order(all_blocks(array, axes, sequence), dim)


def causal_taps(extended, tap_weights, length):
    kernel_len = tap_weights.shape[0]
    summed = jnp.zeros((length,) + extended.shape[1:], jnp.float32)
    for offset in range(kernel_len):
        window_rows = extended[offset : offset + length].astype(jnp.float32)
        summed = summed + tap_weights[offset].astype(jnp.float32) * window_rows
    return jax.nn.silu(summed).astype(jnp.bfloat16)


def block_pass(values, key_rows, queries, step_sizes, decay_rates):
    length, groups, head_count, head_dim = values.shape
    block_count = length // BLOCK
    state_len = key_rows.shape[-1]
    log_decay = -step_sizes * decay_rates
    causal = jnp.tril(jnp.ones((BLOCK, BLOCK), dtype=bool))

    def one_block(carry_state, block):
        block_values, block_keys, block_queries, block_steps, block_decay = block
        cumulative = jnp.cumsum(block_decay, axis=0)
        scores = jnp.einsum(
            "lgn,sgn->gls", block_queries, block_keys, preferred_element_type=jnp.float32
        )
        cum_heads = jnp.transpose(cumulative, (1, 2, 0))
        gap_matrix = cum_heads[:, :, :, None] - cum_heads[:, :, None, :]
        decays = jnp.exp(jnp.where(causal, gap_matrix, -jnp.inf))
        step_heads = jnp.transpose(block_steps, (1, 2, 0))[:, :, None, :]
        weights = (scores[:, None] * decays * step_heads).astype(jnp.bfloat16)
        inside = jnp.einsum(
            "ghls,sghp->lghp", weights, block_values, preferred_element_type=jnp.float32
        )
        carried = jnp.einsum("lgn,ghpn->lghp", block_queries.astype(jnp.float32), carry_state)
        carried = carried * jnp.exp(cumulative)[..., None]
        tail_sum = cumulative[-1]
        scaled = (
            block_values.astype(jnp.float32)
            * (block_steps * jnp.exp(tail_sum - cumulative))[..., None]
        )
        fresh_state = jnp.einsum(
            "lghp,lgn->ghpn",
            scaled.astype(jnp.bfloat16),
            block_keys,
            preferred_element_type=jnp.float32,
        )
        next_state = carry_state * jnp.exp(tail_sum)[..., None, None] + fresh_state
        return (next_state, (inside + carried, cumulative))

    blocked = (
        values.reshape(block_count, BLOCK, groups, head_count, head_dim),
        key_rows.reshape(block_count, BLOCK, groups, state_len),
        queries.reshape(block_count, BLOCK, groups, state_len),
        step_sizes.reshape(block_count, BLOCK, groups, head_count),
        log_decay.reshape(block_count, BLOCK, groups, head_count),
    )
    start_state = jnp.zeros((groups, head_count, head_dim, state_len), jnp.float32)
    end_state, (outputs, cumulative) = lax.scan(one_block, start_state, blocked)
    tail_sums = cumulative[:, -1]
    offsets = jnp.cumsum(tail_sums, axis=0) - tail_sums
    device_cum = (cumulative + offsets[:, None]).reshape(length, groups, head_count)
    return (
        outputs.reshape(length, groups, head_count, head_dim),
        device_cum,
        end_state,
        jnp.sum(tail_sums, axis=0),
    )


def head_group(values, key_rows, queries, step_raw, decay_log):
    length = values.shape[0]
    head_count = step_raw.shape[1]
    groups = key_rows.shape[1]
    per_group = head_count // groups
    head_dim = values.shape[1] // head_count
    step_sizes = jax.nn.softplus(step_raw).reshape(length, groups, per_group)
    decay_rates = jnp.exp(decay_log).reshape(groups, per_group)
    return block_pass(
        values.reshape(length, groups, per_group, head_dim),
        key_rows,
        queries,
        step_sizes,
        decay_rates,
    )


def add_entering(outputs, queries, device_cum, entering):
    extra = jnp.einsum("lgn,ghpn->lghp", queries.astype(jnp.float32), entering)
    return outputs + extra * jnp.exp(device_cum)[..., None]


def unit_rms(values):
    return values * lax.rsqrt(jnp.mean(values * values, axis=-1, keepdims=True) + EPS)


def gate_and_norm(mixed_heads, gate_raw, gain):
    length, groups, per_group, head_dim = mixed_heads.shape
    gated = mixed_heads.reshape(length, -1) * jax.nn.silu(gate_raw.astype(jnp.float32))
    normed = unit_rms(gated.reshape(length, groups * per_group, head_dim))
    return (normed.reshape(length, -1) * gain.astype(jnp.float32)).astype(jnp.bfloat16)


def local(
    residual,
    small_heads,
    large_heads,
    state_keys,
    state_queries,
    small_gate,
    large_gate,
    small_step,
    large_step,
    small_taps,
    large_taps,
    key_taps,
    query_taps,
    small_decay,
    large_decay,
    small_gain,
    large_gain,
    small_out,
    large_out,
    mixer_gain,
    ffn_in_gain,
    gate_proj,
    up_proj,
    down_proj,
    ffn_out_gain,
):
    length = residual.shape[0]
    halo_rows = small_taps.shape[0] - 1
    first_row = length - halo_rows
    previous = passed_along(
        (
            small_heads[first_row:],
            large_heads[first_row:],
            state_keys[first_row:],
            state_queries[first_row:],
        ),
        SP,
        1,
    )
    small_conv = causal_taps(
        jnp.concatenate([previous[0], small_heads], axis=0), small_taps, length
    )
    large_conv = causal_taps(
        jnp.concatenate([previous[1], large_heads], axis=0), large_taps, length
    )
    key_conv = causal_taps(jnp.concatenate([previous[2], state_keys], axis=0), key_taps, length)
    query_conv = causal_taps(
        jnp.concatenate([previous[3], state_queries], axis=0), query_taps, length
    )
    small_out_local, small_cum, small_end, small_total = head_group(
        small_conv, key_conv[:, 0:1], query_conv[:, 0:1], small_step, small_decay
    )
    large_out_local, large_cum, large_end, large_total = head_group(
        large_conv, key_conv[:, 1:2], query_conv[:, 1:2], large_step, large_decay
    )

    def join(earlier, later):
        return (
            earlier[0] * jnp.exp(later[1])[..., None, None] + later[0],
            earlier[1] + later[1],
            earlier[2] * jnp.exp(later[3])[..., None, None] + later[2],
            earlier[3] + later[3],
        )

    identity_parts = (
        jnp.zeros_like(small_end),
        jnp.zeros_like(small_total),
        jnp.zeros_like(large_end),
        jnp.zeros_like(large_total),
    )
    entered = prefix_by_axis(
        (small_end, small_total, large_end, large_total), SP, join, identity_parts
    )
    small_enter = entered[0]
    large_enter = entered[2]
    small_mix = add_entering(small_out_local, query_conv[:, 0:1], small_cum, small_enter)
    large_mix = add_entering(large_out_local, query_conv[:, 1:2], large_cum, large_enter)
    small_normed = gate_and_norm(small_mix, small_gate, small_gain)
    large_normed = gate_and_norm(large_mix, large_gate, large_gain)
    partial_value = jnp.dot(small_normed, small_out, preferred_element_type=jnp.float32)
    partial_value = partial_value + jnp.dot(
        large_normed, large_out, preferred_element_type=jnp.float32
    )
    mix = lax.psum(partial_value.astype(jnp.bfloat16), "tp").astype(jnp.float32)
    mixed = residual.astype(jnp.float32) + unit_rms(mix) * mixer_gain.astype(jnp.float32)
    normed_in = (unit_rms(mixed) * ffn_in_gain.astype(jnp.float32)).astype(jnp.bfloat16)
    pieces = in_one_piece((gate_proj, up_proj), SP, 0, 1)
    gate = jnp.dot(normed_in, pieces[0], preferred_element_type=jnp.float32)
    up_values = jnp.dot(normed_in, pieces[1], preferred_element_type=jnp.float32)
    down_full = gather_axes(down_proj, (("sp_0", "sp_1"), "sp_2"), (0, 1), 0)
    hidden = (jax.nn.silu(gate) * up_values).astype(jnp.bfloat16)
    share = length // lax.axis_size("tp")
    ffn = lax.psum_scatter(
        lax.dot_general(
            hidden, down_full, (((1,), (1,)), ((), ())), preferred_element_type=jnp.float32
        ).astype(jnp.bfloat16),
        "tp",
        scatter_dimension=0,
        tiled=True,
    ).astype(jnp.float32)
    own_rows = lax.dynamic_slice_in_dim(mixed, lax.axis_index("tp") * share, share, 0)
    updated = own_rows + 0.5 * unit_rms(ffn) * ffn_out_gain.astype(jnp.float32)
    return updated.astype(jnp.bfloat16)


def solution(mesh):
    torus = Mesh(mesh.devices.reshape(4, 4, 2, mesh.shape["tp"]), ("sp_0", "sp_1", "sp_2", "tp"))
    in_specs = (
        P(SP, None),
        P(SP, "tp"),
        P(SP, "tp"),
        P(SP, "tp", None),
        P(SP, "tp", None),
        P(SP, "tp"),
        P(SP, "tp"),
        P(SP, "tp"),
        P(SP, "tp"),
        P(None, "tp"),
        P(None, "tp"),
        P(None, "tp", None),
        P(None, "tp", None),
        P("tp"),
        P("tp"),
        P("tp"),
        P("tp"),
        P("tp", None),
        P("tp", None),
        P(),
        P(),
        P(SP, "tp"),
        P(SP, "tp"),
        P(SP, "tp"),
        P(),
    )
    out_specs = P(SP_TP, None)
    return jax.shard_map(local, mesh=torus, in_specs=in_specs, out_specs=out_specs, check_vma=False)
```

profile of v0, /device:TPU:1, one launch (start us, length us, event | category | flops | bytes accessed | tf_op | source)
XLA Modules:
  0.0 482.5 jit_solution(811788357132697715)
XLA Ops:
  9.0 4.6 collective-permute-start
  18.5 3.6 collective-permute-start.2
  41.0 3.1 fusion.118
  49.2 83.8 %while.30 = (s32[]{:T(128)}, f32[1,4,64,128]{3,2,1,0:T(8,128)S(1)}, f32[8,128,1,4,64]{1,0,4,3,2:T(8,128)}, f32[8,128,1,4]{3,1,2,0:T(8,128)}, f32[8,128,1,4]{3,1,...) while((s32[]{:T(128)}, f32[1,4,64,128]{3,2,1,0:T(8,128)S(1)}, ...), condition=%wide.region_2.3_spmd.clone, body=%wide.region_0.2_spmd.clone.sunk | while | flops 30065156 | bytes 1596155 | solution.py:149
  54.6 4.4 dynamic_update_slice.27
  65.1 4.4 dynamic_update_slice.27
  75.6 4.4 dynamic_update_slice.27
  86.0 4.4 dynamic_update_slice.27
  96.5 4.4 dynamic_update_slice.27
  107.0 4.4 dynamic_update_slice.27
  117.5 4.4 dynamic_update_slice.27
  127.9 4.4 dynamic_update_slice.27
  138.7 86.1 %while.31 = (s32[]{:T(128)}, f32[1,2,128,128]{3,2,1,0:T(8,128)S(1)}, f32[8,128,1,2,128]{1,0,4,3,2:T(8,128)}, f32[8,128,1,2]{3,1,2,0:T(8,128)}, f32[8,128,1,2]{3,...) while((s32[]{:T(128)}, ...), condition=%wide.region_5.6_spmd.clone, body=%wide.region_3.5_spmd.clone.sunk | while | flops 29868292 | bytes 1569483 | solution.py:149
  144.1 4.8 dynamic_update_slice.29
  154.9 4.8 dynamic_update_slice.29
  165.7 4.8 dynamic_update_slice.29
  176.4 4.8 dynamic_update_slice.29
  187.2 4.8 dynamic_update_slice.29
  198.0 4.8 dynamic_update_slice.29
  208.7 4.8 dynamic_update_slice.29
  219.5 4.8 dynamic_update_slice.29
  228.6 11.5 %all-gather.6 = bf16[4,514,128]{2,1,0:T(8,128)(2,1)S(1)} all-gather(bf16[1,514,128]{2,1,0:T(8,128)(2,1)S(1)} %maximum_bitcast_fusion.1), channel_id=3, replica_groups=mesh['sp_0'=4,'sp_1'=4,'sp_2'=2,'tp'=4] {'sp_1'}, dimensions={0}, use_global_device_ids=true | all-gather | bytes 657920 | tf_op jit(solution)/shard_map/all_gather | solution.py:33
  241.5 10.9 %all-gather.7 = bf16[4,514,128]{2,1,0:T(8,128)(2,1)S(1)} all-gather(bf16[1,514,128]{2,1,0:T(8,128)(2,1)S(1)} %maximum_bitcast_fusion.2), channel_id=4, replica_groups=mesh['sp_0'=4,'sp_1'=4,'sp_2'=2,'tp'=4] {'sp_0'}, dimensions={0}, use_global_device_ids=true | all-gather | bytes 657920 | tf_op jit(solution)/shard_map/all_gather | solution.py:33
  274.4 3.3 add_convert_fusion
  279.7 94.6 %all-reduce.8.cloned.1.call-done = bf16[1024,2048]{1,0:T(8,128)(2,1)} async-done(((bf16[1024,2048]{1,0:T(8,128)(2,1)}), bf16[1024,2048]{1,0:T(8,128)(2,1)}) %all-reduce.8.cloned.1.call-update) | async-done | bytes 4194320 | tf_op jit(solution)/shard_map/psum | solution.py:278
  374.3 3.2 fusion.74
  377.8 6.0 %multiply_reduce_fusion = (f32[1024]{0:T(1024)S(1)}, f32[1024,2048]{1,0:T(8,128)}) fusion(f32[2048]{0:T(1024)S(1)} %convert_element_type.718, f32[1024]{0:T(1024)S(1)} %add_rsqrt_fusion.3, bf16[1024,2048]{1,0:T(8,128)(2,1)S(1)} %copy-done.2, bf16[1024,2048]{1,0:T(8,128)(2,1)} %param.29), kind=kLoop, calls=%fused_computation.98 | loop fusion | flops 14679040 | bytes 16793600 | tf_op jit(solution)/shard_map/reduce_sum | solution.py:184
  383.8 5.8 %copy.254 = bf16[16,2,64,1408]{3,2,1,0:T(8,128)(2,1)} copy(bf16[16,2,64,1408]{3,2,0,1:T(8,128)(2,1)} %bitcast.557) | data formatting | bytes 11534336 | tf_op jit(solution)/shard_map/transpose | solution.py:87
  389.6 12.6 %fusion.79 = f32[1024,1408]{1,0:T(8,128)} fusion(bf16[2048,2816]{1,0:T(8,128)(2,1)} %all-gather.12.cloned.1.call-done, f32[1024,2048]{1,0:T(8,128)} %get-tuple-element.310, f32[2048]{0:T(1024)S(1)} %convert_element_type.719, f32[1024]{0:T(1024)S(1)} %add_rsqrt_fusion.2), kind=kOutput, calls=%fused_computation.102 | convolution fusion | flops 5911871488 | bytes 19935232 | tf_op jit(solution)/shard_map/dot_general | solution.py:282
  402.2 21.5 %fusion.86 = bf16[1024,2048]{1,0:T(8,128)(2,1)} fusion(bf16[2048,1408]{1,0:T(8,128)(2,1)} %bitcast.558, f32[1024,1408]{1,0:T(8,128)} %fusion.79, bf16[2048,2816]{1,0:T(8,128)(2,1)} %all-gather.12.cloned.1.call-done, f32[1024,2048]{1,0:T(8,128)} %get-tuple-element.310, f32[2048]{0:T(1024)S(1)} %convert_element_type.719, f32[1024]{0:T(1024)S(1)} %add_rsqrt_fusion.2), kind=kOutput, calls=%fused_computation.106 | convolution fusion | flops 11828199424 | bytes 29896704 | tf_op jit(solution)/shard_map/dot_general | solution.py:288
  423.7 46.8 %reduce-scatter.2.cloned.1.call-done = bf16[256,2048]{1,0:T(8,128)(2,1)} async-done(((bf16[1024,2048]{1,0:T(8,128)(2,1)}), bf16[256,2048]{1,0:T(8,128)(2,1)}) %reduce-scatter.2.cloned.1.call-update) | async-done | bytes 1048592 | tf_op jit(solution)/shard_map/reduce_scatter | solution.py:287
  472.1 3.3 fusion.93
  (453 shorter events, 162.4 us)
Async XLA Ops:
  7.4 265.7 %copy-start = (bf16[256,2048]{1,0:T(8,128)(2,1)S(1)}, bf16[256,2048]{1,0:T(8,128)(2,1)}, u32[]{:S(2)}) copy-start(bf16[256,2048]{1,0:T(8,128)(2,1)} %param.46) | copy-start | bytes 3145732
  7.4 31.6 %copy-start.12 = (bf16[256]{0:T(256)(128)(2,1)S(1)}, bf16[256]{0:T(256)(128)(2,1)}, u32[]{:S(2)}) copy-start(bf16[256]{0:T(256)(128)(2,1)} %param.45) | copy-start | bytes 1540
  7.4 270.4 %all-gather.14.cloned.1.call-start = ((), (), s32[]{:S(2)}) async-start(), calls=%async_computation.4 | async-start | bytes 3063808 | tf_op jit(solution)/shard_map/all_gather | solution.py:84
  8.1 366.2 %all-reduce.8.cloned.1.call-start = ((), (), s32[]{:S(2)}) async-start(), calls=%async_computation.1 | async-start | bytes 8388608 | tf_op jit(solution)/shard_map/psum | solution.py:278
  9.0 32.0 %collective-permute-start = (bf16[3,256]{0,1:T(8,128)(2,1)S(1)}, bf16[3,256]{0,1:T(8,128)(2,1)S(1)}, u32[]{:S(2)}, u32[]{:S(2)}) collective-permute-start(bf16[3,256]{0,1:T(8,128)(2,1)S(1)} %copy.225), channel_id=1, source_target_pairs={{0,4},{4,8},{8,12},{12,16},{16,20},{20,24},{24,28},{28,32},{32,36}... | collective-permute-start | bytes 4616 | tf_op jit(solution)/shard_map/ppermute | solution.py:16
  14.7 25.6 %collective-permute-start.1 = (bf16[3,2,128]{2,0,1:T(4,128)(2,1)S(1)}, bf16[3,2,128]{2,0,1:T(4,128)(2,1)S(1)}, u32[]{:S(2)}, u32[]{:S(2)}) collective-permute-start(bf16[3,2,128]{2,0,1:T(4,128)(2,1)S(1)} %slice.452), channel_id=1, source_target_pairs={{0,4},{4,8},{8,12},{12,16},{16,20},{20,24},{24,28},{28,32},{32,36}... | collective-permute-start | bytes 4616 | tf_op jit(solution)/shard_map/ppermute | solution.py:16
  17.7 0.8 copy-start.5
  18.5 27.4 %collective-permute-start.2 = (bf16[3,2,128]{2,0,1:T(4,128)(2,1)S(1)}, bf16[3,2,128]{2,0,1:T(4,128)(2,1)S(1)}, u32[]{:S(2)}, u32[]{:S(2)}) collective-permute-start(bf16[3,2,128]{2,0,1:T(4,128)(2,1)S(1)} %slice.458), channel_id=1, source_target_pairs={{0,4},{4,8},{8,12},{12,16},{16,20},{20,24},{24,28},{28,32},{32,36}... | collective-permute-start | bytes 4616 | tf_op jit(solution)/shard_map/ppermute | solution.py:16
  23.0 111.7 %collective-permute-start.3 = (bf16[3,256]{0,1:T(8,128)(2,1)S(1)}, bf16[3,256]{0,1:T(8,128)(2,1)S(1)}, u32[]{:S(2)}, u32[]{:S(2)}) collective-permute-start(bf16[3,256]{0,1:T(8,128)(2,1)S(1)} %copy.239), channel_id=1, source_target_pairs={{0,4},{4,8},{8,12},{12,16},{16,20},{20,24},{24,28},{28,32},{32,36}... | collective-permute-start | bytes 4616 | tf_op jit(solution)/shard_map/ppermute | solution.py:16
  252.5 0.8 copy-start.4
  266.2 5.7 %copy-start.3 = (f32[1024,1,2,128]{0,3,2,1:T(8,128)S(1)}, f32[1024,1,2,128]{0,3,2,1:T(8,128)}, u32[]{:S(2)}) copy-start(f32[1024,1,2,128]{0,3,2,1:T(8,128)} %reshape.977) | copy-start | bytes 3145732
  272.7 1.7 copy-start.6
  277.6 0.9 copy-start.7
  277.6 1.0 copy-start.8
  277.6 2.1 copy-start.9
  277.6 2.1 copy-start.10
  277.7 106.1 %all-gather.16.cloned.1.call-start = ((), (), s32[]{:S(2)}) async-start(), calls=%async_computation.5 | async-start | bytes 8650752 | tf_op jit(solution)/shard_map/all_gather | solution.py:84
  278.4 111.1 %all-gather.12.cloned.1.call-start = ((), (), s32[]{:S(2)}) async-start(), calls=%async_computation.2 | async-start | bytes 11894784 | tf_op jit(solution)/shard_map/all_gather | solution.py:68
  279.4 191.1 %reduce-scatter.2.cloned.1.call-start = ((), (), s32[]{:S(2)}) async-start(), calls=%async_computation.3 | async-start | bytes 5242880 | tf_op jit(solution)/shard_map/reduce_scatter | solution.py:287
  374.3 3.4 copy-start.2
  402.2 21.6 %copy-start.11 = (bf16[2048]{0:T(1024)(128)(2,1)S(1)}, bf16[2048]{0:T(1024)(128)(2,1)}, u32[]{:S(2)}) copy-start(bf16[2048]{0:T(1024)(128)(2,1)} %param.53) | copy-start | bytes 12292
  402.2 73.2 %copy-start.1 = (bf16[256,2048]{1,0:T(8,128)(2,1)S(1)}, bf16[256,2048]{1,0:T(8,128)(2,1)}, u32[]{:S(2)}) copy-start(bf16[256,2048]{1,0:T(8,128)(2,1)} %param.46) | copy-start | bytes 3145732
Sparse Core Ops, SparseCore 0:
  10.3 49.5 all-gather.13
  280.1 23.3 all-gather.15
  305.8 61.5 all-gather.11
Sparse Core Ops, SparseCore 1:
  277.7 96.5 all-reduce.7
  423.8 46.7 reduce-scatter.1
where the time goes:
time: 490 us; the launch traced here: 482 us
  waiting for transfers between devices  143 us (29%)
  local copies, waits for them, and re-layouts  137 us (28%)
  matrix products  104 us (21%)
  other arithmetic  45 us (9%)
  blocking collectives  24.6 us (5%)
  between operations  15.1 us (3%)
  starting transfers between devices  12.4 us (3%)
    psum x1, waiting for transfers between devices, local(): mix = lax.psum(partial_value.astype(jnp.bfloat16), 'tp').astype(jnp.float32)  94.6 us
    dynamic_update_slice x32, local copies, waits for them, and re-layouts, block_pass(): end_state, (outputs, cumulative) = lax.scan(one_block, start_state, blocked)  83.5 us
    reduce_scatter x1, waiting for transfers between devices, local(): lax.psum_scatter(lax.dot_general(hidden, down_full, (((1,), (1,)), ((), (...  46.8 us
    all_gather x3, blocking collectives, collected_together(): both, at, found = (lax.all_gather(jnp.concatenate(lines), axis), 0, {})  24.6 us
    dot_general x1, matrix products, local(): lax.dot_general(hidden, down_full, (((1,), (1,)), ((), ())), preferred_el...  21.5 us
    dot_general x16, matrix products, one_block(): jnp.einsum('ghls,sghp->lghp', weights, block_values, preferred_element_ty...  17.7 us
    dot_general x16, matrix products, one_block(): jnp.einsum('lghp,lgn->ghpn', scaled.astype(jnp.bfloat16), block_keys, pre...  16.3 us
    dynamic_slice x48, local copies, waits for them, and re-layouts, block_pass(): end_state, (outputs, cumulative) = lax.scan(one_block, start_state, blocked)  15.4 us
  transfers between devices with their start and end apart: 9, of which 2 were waited for; matrix products, arithmetic and copies ran while one was open for 51% of the time, Pallas kernels for 0%

commit v1 on v0

--- a/solution.py
+++ b/solution.py
@@ -8,6 +8,12 @@
 SP = ("sp_0", "sp_1", "sp_2")
 SP_TP = ("sp_0", "sp_1", "sp_2", "tp")
 EPS = 1e-06
+
+
+def summed_here(x, name):
+    parts = lax.all_gather(x, name, axis=0, tiled=False)
+    result = parts.sum(axis=0)
+    return result
 
 
 def passed_along(block, axis, distance):
@@ -275,7 +281,7 @@
     partial_value = partial_value + jnp.dot(
         large_normed, large_out, preferred_element_type=jnp.float32
     )
-    mix = lax.psum(partial_value.astype(jnp.bfloat16), "tp").astype(jnp.float32)
+    mix = summed_here(partial_value.astype(jnp.bfloat16), "tp").astype(jnp.float32)
     mixed = residual.astype(jnp.float32) + unit_rms(mix) * mixer_gain.astype(jnp.float32)
     normed_in = (unit_rms(mixed) * ffn_in_gain.astype(jnp.float32)).astype(jnp.bfloat16)
     pieces = in_one_piece((gate_proj, up_proj), SP, 0, 1)

time: 490 us -> 619 us (1.26)
  waiting for transfers between devices: 143 us -> 239 us
  local copies, waits for them, and re-layouts: 137 us -> 159 us
  other arithmetic: 45 us -> 63.6 us
    all_gather x0 -> x1, waiting for transfers between devices: none -> 151 us  [summed_here(): parts = lax.all_gather(x, name, axis=0, tiled=False)]
    psum x1 -> x0, waiting for transfers between devices: 94.6 us -> none  [local(): mix = lax.psum(partial_value.astype(jnp.bfloat16), 'tp').astype(jnp.float32)]
    all_gather x1, waiting for transfers between devices: 0.01 us -> 42.1 us  [in_one_piece(): lax.all_gather(both, axis, axis=dim, tiled=True)]
    reduce_sum x0 -> x1, other arithmetic: none -> 12.1 us  [summed_here(): result = parts.sum(axis=0)]
    unnamed x42 -> x70, local copies, waits for them, and re-layouts: 12.9 us -> 12.8 us
  transfers between devices with their start and end apart: 9 -> 9, of which waited for: 2 -> 3; matrix products, arithmetic and copies ran while one was open for 51% -> 45% of each run, Pallas kernels for 0% -> 0%
where the time goes in v1:
time: 619 us; the launch traced here: 612 us
  waiting for transfers between devices  239 us (39%)
  local copies, waits for them, and re-layouts  159 us (26%)
  matrix products  98.3 us (16%)
  other arithmetic  63.6 us (10%)
  blocking collectives  24.4 us (4%)
  between operations  13.7 us (2%)
  starting transfers between devices  12.6 us (2%)
    all_gather x1, waiting for transfers between devices, summed_here(): parts = lax.all_gather(x, name, axis=0, tiled=False)  151 us
    dynamic_update_slice x32, local copies, waits for them, and re-layouts, block_pass(): end_state, (outputs, cumulative) = lax.scan(one_block, start_state, blocked)  83.9 us
    reduce_scatter x1, waiting for transfers between devices, local(): lax.psum_scatter(lax.dot_general(hidden, down_full, (((1,), (1,)), ((), (...  45.9 us
    all_gather x1, waiting for transfers between devices, in_one_piece(): lax.all_gather(both, axis, axis=dim, tiled=True)  42.1 us
    all_gather x3, blocking collectives, collected_together(): both, at, found = (lax.all_gather(jnp.concatenate(lines), axis), 0, {})  24.4 us
    dot_general x1, matrix products, local(): lax.dot_general(hidden, down_full, (((1,), (1,)), ((), ())), preferred_el...  21.6 us
    dynamic_slice x48, local copies, waits for them, and re-layouts, block_pass(): end_state, (outputs, cumulative) = lax.scan(one_block, start_state, blocked)  20.6 us
    dot_general x16, matrix products, one_block(): jnp.einsum('ghls,sghp->lghp', weights, block_values, preferred_element_ty...  17.7 us
  transfers between devices with their start and end apart: 9, of which 3 were waited for; matrix products, arithmetic and copies ran while one was open for 45% of the time, Pallas kernels for 0%

profile of v1, /device:TPU:1, one launch (start us, length us, event | category | flops | bytes accessed | tf_op | source)
XLA Modules:
  0.0 611.6 jit_solution(17465058946183061323)
XLA Ops:
  8.6 4.6 collective-permute-start.2
  19.1 3.6 collective-permute-start
  53.8 88.3 %while.30 = (s32[]{:T(128)}, f32[1,4,64,128]{3,2,1,0:T(8,128)S(1)}, f32[8,128,1,4,64]{1,0,4,3,2:T(8,128)}, f32[8,128,1,4]{3,1,2,0:T(8,128)}, f32[8,128,1,4]{3,1,...) while((s32[]{:T(128)}, f32[1,4,64,128]{3,2,1,0:T(8,128)S(1)}, ...), condition=%wide.region_2.3_spmd.clone, body=%wide.region_0.2_spmd.clone.sunk | while | flops 30065156 | bytes 1597160 | solution.py:155
  58.7 4.4 dynamic_update_slice.27
  69.7 4.4 dynamic_update_slice.27
  80.8 4.4 dynamic_update_slice.27
  91.8 4.4 dynamic_update_slice.27
  102.8 4.4 dynamic_update_slice.27
  113.8 4.4 dynamic_update_slice.27
  124.9 4.4 dynamic_update_slice.27
  135.9 4.4 dynamic_update_slice.27
  147.1 90.4 %while.31 = (s32[]{:T(128)}, f32[1,2,128,128]{3,2,1,0:T(8,128)S(1)}, f32[8,128,1,2,128]{1,0,4,3,2:T(8,128)}, f32[8,128,1,2]{3,1,2,0:T(8,128)}, f32[8,128,1,2]{3,...) while((s32[]{:T(128)}, ...), condition=%wide.region_5.6_spmd.clone, body=%wide.region_3.5_spmd.clone.sunk | while | flops 29868292 | bytes 1569980 | solution.py:155
  151.9 4.8 dynamic_update_slice.29
  163.2 4.8 dynamic_update_slice.29
  174.6 4.8 dynamic_update_slice.29
  185.8 4.8 dynamic_update_slice.29
  197.2 4.8 dynamic_update_slice.29
  208.4 4.8 dynamic_update_slice.29
  219.7 4.8 dynamic_update_slice.29
  231.0 4.8 dynamic_update_slice.29
  241.8 10.9 %all-gather.7 = bf16[4,514,128]{2,1,0:T(8,128)(2,1)S(1)} all-gather(bf16[1,514,128]{2,1,0:T(8,128)(2,1)S(1)} %maximum_bitcast_fusion.1), channel_id=3, replica_groups=mesh['sp_0'=4,'sp_1'=4,'sp_2'=2,'tp'=4] {'sp_1'}, dimensions={0}, use_global_device_ids=true | all-gather | bytes 657920 | tf_op jit(solution)/shard_map/all_gather | solution.py:39
  255.1 10.8 %all-gather.8 = bf16[4,514,128]{2,1,0:T(8,128)(2,1)S(1)} all-gather(bf16[1,514,128]{2,1,0:T(8,128)(2,1)S(1)} %maximum_bitcast_fusion.2), channel_id=4, replica_groups=mesh['sp_0'=4,'sp_1'=4,'sp_2'=2,'tp'=4] {'sp_0'}, dimensions={0}, use_global_device_ids=true | all-gather | bytes 657920 | tf_op jit(solution)/shard_map/all_gather | solution.py:39
  294.7 3.3 add_convert_fusion
  299.2 5.7 copy.254
  304.9 151.3 %all-gather.16.cloned.1.call-done = bf16[4096,2048]{1,0:T(8,128)(2,1)} async-done(((bf16[1024,2048]{1,0:T(8,128)(2,1)}), bf16[4096,2048]{1,0:T(8,128)(2,1)}) %all-gather.16.cloned.1.call-update) | async-done | bytes 16777232 | tf_op jit(solution)/shard_map/all_gather | solution.py:14
  456.2 12.1 %reduce_sum.79 = bf16[1024,2048]{1,0:T(8,128)(2,1)} reduce(bf16[4,1024,2048]{2,1,0:T(8,128)(2,1)} %bitcast.555, bf16[]{:T(256)} %constant.118.clone.1), dimensions={0}, to_apply=%region_12.13 | reduce | flops 6291456 | bytes 20971522 | tf_op jit(solution)/shard_map/reduce_sum | solution.py:15
  468.3 3.4 fusion.74
  472.1 6.0 multiply_reduce_fusion
  478.1 42.1 %all-gather.14.cloned.1.call-done = bf16[2048,2816]{1,0:T(8,128)(2,1)} async-done(((bf16[64,2816]{1,0:T(8,128)(2,1)}), bf16[2048,2816]{1,0:T(8,128)(2,1)}) %all-gather.14.cloned.1.call-update) | async-done | bytes 11534352 | tf_op jit(solution)/shard_map/all_gather | solution.py:74
  520.2 12.5 %fusion.79 = f32[1024,1408]{1,0:T(8,128)} fusion(bf16[2048,2816]{1,0:T(8,128)(2,1)} %all-gather.14.cloned.1.call-done, f32[1024,2048]{1,0:T(8,128)} %get-tuple-element.310, f32[2048]{0:T(1024)S(1)} %convert_element_type.721, f32[1024]{0:T(1024)S(1)} %add_rsqrt_fusion.2), kind=kOutput, calls=%fused_computation.102 | convolution fusion | flops 5911871488 | bytes 19935232 | tf_op jit(solution)/shard_map/dot_general | solution.py:288
  532.8 21.6 %fusion.86 = bf16[1024,2048]{1,0:T(8,128)(2,1)} fusion(bf16[2048,1408]{1,0:T(8,128)(2,1)} %bitcast.560, f32[1024,1408]{1,0:T(8,128)} %fusion.79, bf16[2048,2816]{1,0:T(8,128)(2,1)} %all-gather.14.cloned.1.call-done, f32[1024,2048]{1,0:T(8,128)} %get-tuple-element.310, f32[2048]{0:T(1024)S(1)} %convert_element_type.721, f32[1024]{0:T(1024)S(1)} %add_rsqrt_fusion.2), kind=kOutput, calls=%fused_computation.106 | convolution fusion | flops 11828199424 | bytes 29896704 | tf_op jit(solution)/shard_map/dot_general | solution.py:294
  554.4 45.9 %reduce-scatter.2.cloned.1.call-done = bf16[256,2048]{1,0:T(8,128)(2,1)} async-done(((bf16[1024,2048]{1,0:T(8,128)(2,1)}), bf16[256,2048]{1,0:T(8,128)(2,1)}) %reduce-scatter.2.cloned.1.call-update) | async-done | bytes 1048592 | tf_op jit(solution)/shard_map/reduce_scatter | solution.py:293
  (482 shorter events, 189.8 us)
Async XLA Ops:
  6.5 286.8 %copy-start = (bf16[256,2048]{1,0:T(8,128)(2,1)S(1)}, bf16[256,2048]{1,0:T(8,128)(2,1)}, u32[]{:S(2)}) copy-start(bf16[256,2048]{1,0:T(8,128)(2,1)} %param.46) | copy-start | bytes 3145732
  6.5 34.0 %copy-start.8 = (bf16[1024,256]{1,0:T(8,128)(2,1)S(1)}, bf16[1024,256]{1,0:T(8,128)(2,1)}, u32[]{:S(2)}) copy-start(bf16[1024,256]{1,0:T(8,128)(2,1)} %param.35) | copy-start | bytes 1572868
  6.5 34.3 %copy-start.25 = (bf16[256]{0:T(256)(128)(2,1)S(1)}, bf16[256]{0:T(256)(128)(2,1)}, u32[]{:S(2)}) copy-start(bf16[256]{0:T(256)(128)(2,1)} %param.45) | copy-start | bytes 1540
  6.5 36.1 %copy-start.26 = (bf16[256]{0:T(256)(128)(2,1)S(1)}, bf16[256]{0:T(256)(128)(2,1)}, u32[]{:S(2)}) copy-start(bf16[256]{0:T(256)(128)(2,1)} %param.44) | copy-start | bytes 1540
  6.5 266.7 %all-gather.18.cloned.1.call-start = ((), (), s32[]{:S(2)}) async-start(), calls=%async_computation.4 | async-start | bytes 3063808 | tf_op jit(solution)/shard_map/all_gather | solution.py:90
  8.6 34.5 %collective-permute-start.2 = (bf16[3,2,128]{2,0,1:T(4,128)(2,1)S(1)}, bf16[3,2,128]{2,0,1:T(4,128)(2,1)S(1)}, u32[]{:S(2)}, u32[]{:S(2)}) collective-permute-start(bf16[3,2,128]{2,0,1:T(4,128)(2,1)S(1)} %slice.458), channel_id=1, source_target_pairs={{0,4},{4,8},{8,12},{12,16},{16,20},{20,24},{24,28},{28,32},{32,36}... | collective-permute-start | bytes 4616 | tf_op jit(solution)/shard_map/ppermute | solution.py:22
  15.7 30.6 %collective-permute-start.1 = (bf16[3,2,128]{2,0,1:T(4,128)(2,1)}, bf16[3,2,128]{2,0,1:T(4,128)(2,1)}, u32[]{:S(2)}, u32[]{:S(2)}) collective-permute-start(bf16[3,2,128]{2,0,1:T(4,128)(2,1)} %slice.452), channel_id=1, source_target_pairs={{0,4},{4,8},{8,12},{12,16},{16,20},{20,24},{24,28},{28,32},{32,36}... | collective-permute-start | bytes 4616 | tf_op jit(solution)/shard_map/ppermute | solution.py:22
  19.1 30.6 %collective-permute-start = (bf16[3,256]{0,1:T(8,128)(2,1)}, bf16[3,256]{0,1:T(8,128)(2,1)}, u32[]{:S(2)}, u32[]{:S(2)}) collective-permute-start(bf16[3,256]{0,1:T(8,128)(2,1)} %copy.225), channel_id=1, source_target_pairs={{0,4},{4,8},{8,12},{12,16},{16,20},{20,24},{24,28},{28,32},{32,36}... | collective-permute-start | bytes 4616 | tf_op jit(solution)/shard_map/ppermute | solution.py:22
  24.1 118.7 %collective-permute-start.3 = (bf16[3,256]{0,1:T(8,128)(2,1)}, bf16[3,256]{0,1:T(8,128)(2,1)}, u32[]{:S(2)}, u32[]{:S(2)}) collective-permute-start(bf16[3,256]{0,1:T(8,128)(2,1)} %copy.239), channel_id=1, source_target_pairs={{0,4},{4,8},{8,12},{12,16},{16,20},{20,24},{24,28},{28,32},{32,36}... | collective-permute-start | bytes 4616 | tf_op jit(solution)/shard_map/ppermute | solution.py:22
  26.1 273.2 %all-gather.20.cloned.1.call-start = ((), (), s32[]{:S(2)}) async-start(), calls=%async_computation.5 | async-start | bytes 8650752 | tf_op jit(solution)/shard_map/all_gather | solution.py:90
  254.6 26.0 %copy-start.11 = (f32[256]{0:T(256)}, f32[256]{0:T(256)S(1)}, u32[]{:S(2)}) copy-start(f32[256]{0:T(256)S(1)} %broadcast_bitcast_fusion.7) | copy-start | bytes 3076
  254.7 25.9 %copy-start.12 = (f32[256]{0:T(256)}, f32[256]{0:T(256)S(1)}, u32[]{:S(2)}) copy-start(f32[256]{0:T(256)S(1)} %broadcast_bitcast_fusion.8) | copy-start | bytes 3076
  254.8 25.8 %copy-start.13 = (f32[256]{0:T(256)}, f32[256]{0:T(256)S(1)}, u32[]{:S(2)}) copy-start(f32[256]{0:T(256)S(1)} %broadcast_bitcast_fusion.9) | copy-start | bytes 3076
  255.1 21.2 %copy-start.24 = (f32[1,4]{1,0:T(1,128)S(1)}, f32[1,4]{1,0:T(1,128)}, u32[]{:S(2)}) copy-start(f32[1,4]{1,0:T(1,128)} %get-tuple-element.315) | copy-start | bytes 52
  273.3 183.0 %all-gather.16.cloned.1.call-start = ((), (), s32[]{:S(2)}) async-start(), calls=%async_computation.3 | async-start | bytes 20971520 | tf_op jit(solution)/shard_map/all_gather | solution.py:14
  284.2 6.4 %copy-start.14 = (f32[256]{0:T(256)S(1)}, f32[256]{0:T(256)}, u32[]{:S(2)}) copy-start(f32[256]{0:T(256)} %mul.1072) | copy-start | bytes 3076
  284.2 6.5 %copy-start.15 = (f32[256]{0:T(256)S(1)}, f32[256]{0:T(256)}, u32[]{:S(2)}) copy-start(f32[256]{0:T(256)} %mul.1076) | copy-start | bytes 3076
  284.2 6.5 %copy-start.16 = (f32[256]{0:T(256)S(1)}, f32[256]{0:T(256)}, u32[]{:S(2)}) copy-start(f32[256]{0:T(256)} %mul.1081) | copy-start | bytes 3076
  284.2 6.5 %copy-start.17 = (f32[256]{0:T(256)S(1)}, f32[256]{0:T(256)}, u32[]{:S(2)}) copy-start(f32[256]{0:T(256)} %mul.1086) | copy-start | bytes 3076
  284.2 6.5 %copy-start.18 = (f32[256]{0:T(256)S(1)}, f32[256]{0:T(256)}, u32[]{:S(2)}) copy-start(f32[256]{0:T(256)} %mul.1103) | copy-start | bytes 3076
  284.2 6.5 %copy-start.19 = (f32[256]{0:T(256)S(1)}, f32[256]{0:T(256)}, u32[]{:S(2)}) copy-start(f32[256]{0:T(256)} %mul.1091) | copy-start | bytes 3076
  284.2 8.0 %copy-start.3 = (f32[1024,1,4,64]{0,3,2,1:T(8,128)S(1)}, f32[1024,1,4,64]{0,3,2,1:T(8,128)}, u32[]{:S(2)}) copy-start(f32[1024,1,4,64]{0,3,2,1:T(8,128)} %reshape.954) | copy-start | bytes 3145732
  286.0 6.9 %copy-start.23 = (f32[256]{0:T(256)S(1)}, f32[256]{0:T(256)}, u32[]{:S(2)}) copy-start(f32[256]{0:T(256)} %convert_element_type.699) | copy-start | bytes 3076
  294.7 3.4 copy-start.9
  294.7 3.4 copy-start.10
  294.7 4.5 copy-start.20
  294.7 4.5 copy-start.21
  298.0 222.2 %all-gather.14.cloned.1.call-start = ((), (), s32[]{:S(2)}) async-start(), calls=%async_computation.1 | async-start | bytes 11894784 | tf_op jit(solution)/shard_map/all_gather | solution.py:74
  298.9 301.4 %reduce-scatter.2.cloned.1.call-start = ((), (), s32[]{:S(2)}) async-start(), calls=%async_computation.2 | async-start | bytes 5242880 | tf_op jit(solution)/shard_map/reduce_scatter | solution.py:293
  468.3 3.8 copy-start.2
  532.8 21.7 %copy-start.22 = (bf16[2048]{0:T(1024)(128)(2,1)S(1)}, bf16[2048]{0:T(1024)(128)(2,1)}, u32[]{:S(2)}) copy-start(bf16[2048]{0:T(1024)(128)(2,1)} %param.53) | copy-start | bytes 12292
  532.8 72.3 %copy-start.1 = (bf16[256,2048]{1,0:T(8,128)(2,1)S(1)}, bf16[256,2048]{1,0:T(8,128)(2,1)}, u32[]{:S(2)}) copy-start(bf16[256,2048]{1,0:T(8,128)(2,1)} %param.46) | copy-start | bytes 3145732
  (4 other events, 4.1 us)
Sparse Core Ops, SparseCore 0:
  26.2 47.8 all-gather.17
  273.4 23.3 all-gather.19
  298.5 157.7 all-gather.15
  458.4 61.8 all-gather.13
  554.5 45.7 reduce-scatter.1
